TPU v7x, 256 devices: a whole 4x4x8 slice. The times are simulated.
256 devices in a mesh: sp: 32 (over z, x), tp: 8 (over y, core).
Axes of the slice: x: 4, y: 4, z: 8, core: 2. Of those that a mesh axis runs over, the one named last changes fastest.
Arguments:
- stream: bfloat16 [32768, 2048], P(('sp', 'tp')), may hold values from -6 to 6
- mixer_input: bfloat16 [32768, 1024], P('sp', 'tp'), may hold values from -6 to 6
- document_ids: int32 [32768], P('sp'), may hold values from 0 to 15, never falling along the last dimension, each value on 1 to 4096 neighbouring positions
- decay_rate: float32 [64, 64], P('tp'), may hold values from 6.1035156e-05 to 0.015625
- rotation: float32 [64, 64], P('tp'), may hold values from -3.140625 to 3.140625
- forget_log: float32 [32768, 64], P('sp', 'tp'), may hold values from -1 to 0
- input_map: bfloat16 [2, 64, 64, 16], P(None, 'tp'), may hold values from -1.5 to 1.5
- readout_map: bfloat16 [2, 64, 16, 64], P(None, 'tp'), may hold values from -0.5 to 0.5
- skip_gain: float32 [64, 16], P('tp'), may hold values from -3 to 3
- out_projection: bfloat16 [1024, 2048], replicated, may hold values from -0.1875 to 0.1875
- norm_gain: float32 [2048], replicated, may hold values from 0.1 to 1.9
- expert_ids: int32 [32768, 8], P('sp'), may hold values from 0 to 255, all different within a row; in each aligned block of 1024 rows (0 to 1023, 1024 to 2047, ...) at most 64 rows name the same one
- route_weight: float32 [32768, 8], P('sp'), may hold values from 0.05 to 1
- expert_gate: bfloat16 [256, 2048, 512], P(('sp', 'tp')), may hold values from -0.125 to 0.125
- expert_up: bfloat16 [256, 2048, 512], P(('sp', 'tp')), may hold values from -0.125 to 0.125
- expert_down: bfloat16 [256, 512, 2048], P(('sp', 'tp')), may hold values from -0.25 to 0.25
- shared_gate: bfloat16 [2048, 512], P(None, 'tp'), may hold values from -0.125 to 0.125
- shared_up: bfloat16 [2048, 512], P(None, 'tp'), may hold values from -0.125 to 0.125
- shared_down: bfloat16 [512, 2048], P('tp'), may hold values from -0.25 to 0.25
Outputs:
- layer_out: bfloat16 [32768, 2048], P(('sp', 'tp'))
Inputs may be any that keep to these rules, and one draw needn't show every extreme that they name: `expert_ids`: each row names 8 different experts. In the rows of one device (aligned blocks of 1024 rows) no expert is named by more than 64 rows. `document_ids`: never falling along the positions; each document covers 1 to 4096 positions.
All inputs are finite; a program needn't handle non-finite values.
Results may differ from a plain program's by a relative error of at most 0.018.
Values may be sent and summed in bfloat16 or wider, within the bound.
A program may use at most 256 MiB of HBM per device.

v0:
```python
import jax
import jax.numpy as jnp
from jax import lax
from jax.sharding import PartitionSpec as P

norm_eps = 1e-06
highest = lax.Precision.HIGHEST
block_span = 16


def from_everyone(array, axis):
    peers = lax.axis_size(axis)
    return lax.all_to_all(
        jnp.broadcast_to(array[None], (peers, *array.shape)), axis, 0, 0, tiled=True
    )


def collected_together(array, axis):
    leaves = jax.tree.leaves(array)
    sequence = sorted(range(len(leaves)), key=lambda k: -leaves[k].size)
    width = (1, *leaves[sequence[0]].shape)[-1]
    lines = [
        jnp.pad(leaves[k].reshape(-1), (0, -leaves[k].size % width)).reshape(-1, width)
        for k in sequence
    ]
    both, at, found = (from_everyone(jnp.concatenate(lines), axis), 0, {})
    for k, line in zip(sequence, lines):
        piece = both[:, at : at + len(line)].reshape(len(both), -1)
        found[k] = piece[:, : leaves[k].size].reshape(-1, *leaves[k].shape)
        at += len(line)
    numbers = iter(range(len(leaves)))
    return jax.tree.map(lambda _: found[next(numbers)], array)


def folded_in_pairs(pieces, combine):
    while len(jax.tree.leaves(pieces)[0]) > 1:
        pieces = jax.vmap(combine)(
            *(jax.tree.map(lambda part: part[side::2], pieces) for side in (0, 1))
        )
    return jax.tree.map(lambda part: part[0], pieces)


def carried_in(array, axis, combine, identity):
    peers, mine = (lax.axis_size(axis), lax.axis_index(axis))
    passed = jnp.arange(peers) < mine

    def kept(part, zero, own):
        part = jnp.where(
            passed.reshape(-1, *(1 for _ in own.shape)), part, jnp.asarray(zero, own.dtype)
        )
        return part

    pieces = collected_together(array, axis)
    return folded_in_pairs(jax.tree.map(kept, pieces, identity, array), combine)


def pair_combine(earlier, later):
    a_re1, a_im1, b_re1, b_im1 = earlier
    a_re2, a_im2, b_re2, b_im2 = later
    return (
        a_re1 * a_re2 - a_im1 * a_im2,
        a_re1 * a_im2 + a_im1 * a_re2,
        a_re2 * b_re1 - a_im2 * b_im1 + b_re2,
        a_re2 * b_im1 + a_im2 * b_re1 + b_im2,
    )


def carry_combine(earlier, later):
    joined = (earlier[5] == later[4]) | (earlier[5] < 0.0) | (later[4] < 0.0)
    merged = pair_combine(earlier[:4], later[:4])
    decay_re = jnp.where(joined, merged[0], 0.0)
    decay_im = jnp.where(joined, merged[1], 0.0)
    state_re = jnp.where(joined, merged[2], later[2])
    state_im = jnp.where(joined, merged[3], later[3])
    first_doc = jnp.where(earlier[4] < 0.0, later[4], earlier[4])
    last_doc = jnp.where(later[5] < 0.0, earlier[5], later[5])
    return (decay_re, decay_im, state_re, state_im, first_doc, last_doc)


def shift_down(values, lag):
    if lag == 0:
        return values
    widths = [(0, 0), (lag, 0)] + [(0, 0)] * (values.ndim - 2)
    return jnp.pad(values[:, : values.shape[1] - lag], widths)


def blocked_states(driven, starts, forget_log, decay_rate, rotation):
    positions, groups_here = forget_log.shape
    states = decay_rate.shape[1]
    blocks = positions // block_span
    cum_log = jnp.cumsum(forget_log.reshape(blocks, block_span, groups_here), axis=1)
    pos_index = jnp.arange(positions, dtype=jnp.int32)
    latest = lax.cummax(jnp.where(starts, pos_index, -1), axis=0).reshape(blocks, block_span)
    pos_blocks = pos_index.reshape(blocks, block_span)
    offsets_in = jnp.arange(block_span, dtype=jnp.int32)
    drive_re = driven[0].reshape(blocks, block_span, groups_here, states)
    drive_im = driven[1].reshape(blocks, block_span, groups_here, states)
    acc_re = jnp.zeros_like(drive_re)
    acc_im = jnp.zeros_like(drive_im)
    for lag in range(block_span):
        src_re = shift_down(drive_re, lag)
        src_im = shift_down(drive_im, lag)
        src_log = shift_down(cum_log, lag)
        valid = (offsets_in[None, :] >= lag) & (latest <= pos_blocks - lag)
        span_gain = jnp.where(valid[:, :, None], jnp.exp(cum_log - src_log), 0.0)
        kern_mag = jnp.exp(-float(lag) * decay_rate)
        kern_re = kern_mag * jnp.cos(float(lag) * rotation)
        kern_im = kern_mag * jnp.sin(float(lag) * rotation)
        coef_re = span_gain[..., None] * kern_re[None, None]
        coef_im = span_gain[..., None] * kern_im[None, None]
        acc_re = acc_re + coef_re * src_re - coef_im * src_im
        acc_im = acc_im + coef_re * src_im + coef_im * src_re
    steps = (offsets_in + 1).astype(jnp.float32)
    enter_mag = jnp.exp(cum_log[..., None] - steps[None, :, None, None] * decay_rate[None, None])
    enter_ok = (latest < pos_blocks[:, :1])[:, :, None, None]
    turn = steps[:, None, None] * rotation[None]
    enter_re = jnp.where(enter_ok, enter_mag * jnp.cos(turn)[None], 0.0)
    enter_im = jnp.where(enter_ok, enter_mag * jnp.sin(turn)[None], 0.0)
    flat = groups_here * states
    scanned = lax.associative_scan(
        pair_combine,
        (
            enter_re[:, -1].reshape(blocks, flat),
            enter_im[:, -1].reshape(blocks, flat),
            acc_re[:, -1].reshape(blocks, flat),
            acc_im[:, -1].reshape(blocks, flat),
        ),
        axis=0,
    )
    ones_row = jnp.ones((1, flat), jnp.float32)
    zero_row = jnp.zeros((1, flat), jnp.float32)
    prev = [
        jnp.concatenate([first_row, member[:-1]]).reshape(blocks, 1, groups_here, states)
        for first_row, member in zip((ones_row, zero_row, zero_row, zero_row), scanned)
    ]
    local_re = acc_re + enter_re * prev[2] - enter_im * prev[3]
    local_im = acc_im + enter_re * prev[3] + enter_im * prev[2]
    prefix_re = enter_re * prev[0] - enter_im * prev[1]
    prefix_im = enter_re * prev[1] + enter_im * prev[0]
    return tuple(
        (member.reshape(positions, flat) for member in (prefix_re, prefix_im, local_re, local_im))
    )


def body(
    stream,
    mixer_input,
    document_ids,
    decay_rate,
    rotation,
    forget_log,
    input_map,
    readout_map,
    skip_gain,
    out_projection,
    norm_gain,
    expert_ids,
    route_weight,
    expert_gate,
    expert_up,
    expert_down,
    shared_gate,
    shared_up,
    shared_down,
):
    positions = mixer_input.shape[0]
    groups_here, states = decay_rate.shape
    group_size = skip_gain.shape[1]
    input_grouped = mixer_input.reshape(positions, groups_here, group_size)
    driven = jnp.einsum(
        "tgh,cgph->ctgp", input_grouped, input_map, preferred_element_type=jnp.float32
    )
    in_scale = jnp.sqrt(1.0 - jnp.exp(-2.0 * decay_rate))
    driven = driven * in_scale[None, None]
    starts = jnp.concatenate([jnp.zeros((1,), bool), document_ids[1:] != document_ids[:-1]])
    prefix_re, prefix_im, local_re, local_im = blocked_states(
        driven, starts, forget_log, decay_rate, rotation
    )
    first_doc = document_ids[:1].astype(jnp.float32)
    summary = (
        prefix_re[-1],
        prefix_im[-1],
        local_re[-1],
        local_im[-1],
        first_doc,
        document_ids[-1:].astype(jnp.float32),
    )
    flat_states = groups_here * states
    identity = (
        jnp.ones((flat_states,), jnp.float32),
        jnp.zeros((flat_states,), jnp.float32),
        jnp.zeros((flat_states,), jnp.float32),
        jnp.zeros((flat_states,), jnp.float32),
        -jnp.ones((1,), jnp.float32),
        -jnp.ones((1,), jnp.float32),
    )
    state_passed = carried_in(summary, "sp", carry_combine, identity)
    same_doc = state_passed[5] == first_doc
    state_re = local_re + jnp.where(
        same_doc, prefix_re * state_passed[2][None] - prefix_im * state_passed[3][None], 0.0
    )
    state_im = local_im + jnp.where(
        same_doc, prefix_re * state_passed[3][None] + prefix_im * state_passed[2][None], 0.0
    )
    readout = (
        jnp.einsum(
            "tgp,ghp->tgh",
            state_re.reshape(positions, groups_here, states),
            readout_map[0].astype(jnp.float32),
            precision=highest,
        )
        - jnp.einsum(
            "tgp,ghp->tgh",
            state_im.reshape(positions, groups_here, states),
            readout_map[1].astype(jnp.float32),
            precision=highest,
        )
        + skip_gain[None] * input_grouped.astype(jnp.float32)
    )
    mixer_out = (
        jax.nn.gelu(readout).reshape(positions, groups_here * group_size).astype(jnp.bfloat16)
    )
    whole_rows = lax.all_to_all(mixer_out, "tp", split_axis=0, concat_axis=1, tiled=True)
    mixed = jnp.dot(whole_rows, out_projection, preferred_element_type=jnp.float32)
    residual = (stream.astype(jnp.float32) + mixed).astype(jnp.bfloat16)
    resid_f = residual.astype(jnp.float32)
    normed = (
        resid_f
        * lax.rsqrt(jnp.mean(resid_f * resid_f, axis=-1, keepdims=True) + norm_eps)
        * norm_gain[None, :]
    ).astype(jnp.bfloat16)
    full_rows = lax.all_gather(normed, "tp", axis=0, tiled=True)
    sp_count = lax.axis_size("sp")
    tp_count = lax.axis_size("tp")
    token_count, route_count = expert_ids.shape
    model_width = full_rows.shape[1]
    capacity = max(2, 2 * token_count * route_count // (sp_count * tp_count))
    column = lax.axis_index("tp")
    flat_expert = expert_ids.reshape(-1)
    flat_token = jnp.arange(token_count * route_count, dtype=jnp.int32) // route_count
    target = flat_expert // tp_count
    is_mine = flat_expert % tp_count == column
    onehot = (
        (target[:, None] == jnp.arange(sp_count, dtype=jnp.int32)[None, :]) & is_mine[:, None]
    ).astype(jnp.int32)
    slot_rank = jnp.sum((jnp.cumsum(onehot, axis=0) - onehot) * onehot, axis=1)
    slot_index = jnp.where(is_mine, target * capacity + slot_rank, sp_count * capacity)
    token_table = (
        jnp.full((sp_count * capacity,), token_count, jnp.int32)
        .at[slot_index]
        .set(flat_token, mode="drop")
    )
    weight_table = (
        jnp.zeros((sp_count * capacity,), jnp.float32)
        .at[slot_index]
        .set(route_weight.reshape(-1), mode="drop")
    )
    padded = jnp.concatenate([full_rows, jnp.zeros((1, model_width), jnp.bfloat16)])
    outbound = padded[token_table].reshape(sp_count, capacity, model_width)
    arrived = lax.all_to_all(outbound, "sp", split_axis=0, concat_axis=0, tiled=True)
    row_block = arrived.reshape(-1, model_width)
    gate_value = jnp.dot(row_block, expert_gate[0], preferred_element_type=jnp.float32)
    up_value = jnp.dot(row_block, expert_up[0], preferred_element_type=jnp.float32)
    hidden = (jax.nn.silu(gate_value) * up_value).astype(jnp.bfloat16)
    expert_rows = jnp.dot(hidden, expert_down[0], preferred_element_type=jnp.float32).astype(
        jnp.bfloat16
    )
    returned = lax.all_to_all(
        expert_rows.reshape(arrived.shape), "sp", split_axis=0, concat_axis=0, tiled=True
    )
    routed = (
        jnp.zeros((token_count, model_width), jnp.float32)
        .at[token_table]
        .add(
            weight_table[:, None] * returned.reshape(-1, model_width).astype(jnp.float32),
            mode="drop",
        )
    )
    gate_block = jnp.dot(full_rows, shared_gate, preferred_element_type=jnp.float32)
    up_block = jnp.dot(full_rows, shared_up, preferred_element_type=jnp.float32)
    shared_hidden = (jax.nn.silu(gate_block) * up_block).astype(jnp.bfloat16)
    partial_value = routed + jnp.dot(shared_hidden, shared_down, preferred_element_type=jnp.float32)
    expert_sum = lax.psum_scatter(
        partial_value.astype(jnp.bfloat16), "tp", scatter_dimension=0, tiled=True
    ).astype(jnp.float32)
    return (resid_f + expert_sum).astype(jnp.bfloat16)


def solution(mesh):
    placed = (
        P(("sp", "tp"), None),
        P("sp", "tp"),
        P("sp"),
        P("tp", None),
        P("tp", None),
        P("sp", "tp"),
        P(None, "tp", None, None),
        P(None, "tp", None, None),
        P("tp", None),
        P(),
        P(),
        P("sp", None),
        P("sp", None),
        P(("sp", "tp"), None, None),
        P(("sp", "tp"), None, None),
        P(("sp", "tp"), None, None),
        P(None, "tp"),
        P(None, "tp"),
        P("tp", None),
    )
    return jax.shard_map(
        body, mesh=mesh, in_specs=placed, out_specs=P(("sp", "tp"), None), check_vma=False
    )
```

profile of v0, /device:TPU:4, one launch (start us, length us, event | category | flops | bytes accessed | tf_op | source)
XLA Modules:
  0.0 925.7 jit_solution(17095378466501293667)
XLA Ops:
  119.5 33.5 %fusion.63 = f32[64,16,8,64]{3,2,1,0:T(8,128)} fusion(f32[64,4,8,64]{3,2,1,0:T(8,128)} %slice.1064, f32[64,3,8,64]{3,2,1,0:T(8,128)} %slice.1068, f32[64,3,8,64]{3,2,1,0:T(8,128)} %slice.1067, f32[64,2,8,64]{3,2,1,0:T(8,128)} %slice.1071, f32[64,2,8,64]{3,2,1,0:T(8,128)} %slice.1070, f32[64,1,8,64]{3,2,1,0:T(8,128)} %slice.1074, ...), kind=kLoop, calls=%fused_computation.137 | loop fusion | flops 49807360 | bytes 38338560 | tf_op jit(solution)/shard_map/add | solution.py:112
  153.0 33.4 %fusion.56 = f32[64,16,8,64]{3,2,1,0:T(8,128)} fusion(f32[64,4,8,64]{3,2,1,0:T(8,128)} %slice.1065, f32[64,3,8,64]{3,2,1,0:T(8,128)} %slice.1067, f32[64,3,8,64]{3,2,1,0:T(8,128)} %slice.1068, f32[64,2,8,64]{3,2,1,0:T(8,128)} %slice.1070, f32[64,2,8,64]{3,2,1,0:T(8,128)} %slice.1071, f32[64,1,8,64]{3,2,1,0:T(8,128)} %slice.1073, ...), kind=kLoop, calls=%fused_computation.130 | loop fusion | flops 49807360 | bytes 38338560 | tf_op jit(solution)/shard_map/sub | solution.py:111
  206.9 5.2 mul.1832
  214.3 4.8 mul.1839
  219.1 10.2 %multiply_subtract_fusion = (f32[64,16,8,64]{3,2,1,0:T(8,128)}, f32[64,16,8,64]{3,2,1,0:T(8,128)}, f32[64,16,8,64]{3,2,1,0:T(8,128)}, f32[64,16,8,64]{3,2,1,0:T(8,128)}) fusion(f32[64,16,8,64]{3,2,1,0:T(8,128)} %fusion.56, f32[64,8,64]{2,1,0:T(8,128)S(1)} %mul.1804, f32[64,8,64]{2,1,0:T(8,128)} %mul.1799, f32[16,8,64]{2,1,0:T(8,128)S(1)} %get-tuple-element.174, ...), kind=kLoop, calls=%fused_computation.154 | loop fusion | flops 6815744 | bytes 12977152 | tf_op jit(solution)/shard_map/sub | solution.py:136
  238.9 4.8 reshape.1317
  254.3 11.6 %all-to-all-start = ((f32[32,6,512]{2,1,0:T(8,128)}), f32[32,6,512]{2,1,0:T(8,128)}, u32[]{:S(2)}, u32[]{:S(2)}) async-start(f32[32,6,512]{2,1,0:T(8,128)} %broadcast_in_dim.456), calls=%async_computation | async-start | bytes 1048576 | tf_op jit(solution)/shard_map/all_to_all | solution.py:13
  266.0 16.8 %all-to-all-done = f32[32,6,512]{2,1,0:T(8,128)} async-done(((f32[32,6,512]{2,1,0:T(8,128)}), f32[32,6,512]{2,1,0:T(8,128)}, u32[]{:S(2)}, u32[]{:S(2)}) %all-to-all-start) | async-done | bytes 393248 | tf_op jit(solution)/shard_map/all_to_all | solution.py:13
  332.6 8.1 bitcast_add_fusion.1
  345.9 11.8 %all_to_all.31 = bf16[8,128,128]{1,2,0:T(8,128)(2,1)S(1)} all-to-all(bf16[8,128,128]{1,2,0:T(8,128)(2,1)S(1)} %copy.231), channel_id=1, replica_groups=mesh['sp'=32,'tp'=8] {'tp'}, dimensions={0} | all-to-all | bytes 524288 | tf_op jit(solution)/shard_map/all_to_all | solution.py:223
  362.6 17.2 %reduce-window.19 = s32[32,64,128]{2,1,0:T(8,128)S(1)} reduce-window(s32[32,64,128]{2,1,0:T(8,128)} %fusion.97, s32[]{:T(128)} %constant.240.clone.1), window={size=1x1x128 pad=0_0x0_0x127_0}, to_apply=%region_4.5 | reduce-window | flops 33292288 | bytes 2097156 | tf_op jit(solution)/shard_map/reduce-window.2
  382.5 30.7 %scatter_custom_fusion = s32[2048]{0:T(1024)S(1)} fusion(s32[8192]{0:T(1024)S(1)} %bitcast.284, s32[8192]{0:T(1024)S(1)} %add_select_fusion, s32[]{:T(128)} %constant.239.clone.1), kind=kCustom, calls=%fused_computation.414 | custom fusion | bytes 8196 | tf_op jit(solution)/shard_map/scatter | solution.py:251
  413.2 4.9 concatenate.110
  418.1 19.1 %gather_fusion = bf16[2048,2048]{1,0:T(8,128)(2,1)} fusion(bf16[1025,2048]{1,0:T(8,128)(2,1)} %concatenate.110, s32[2048]{0:T(1024)S(1)} %get-tuple-element.131), kind=kCustom, calls=%fused_computation | custom fusion | bytes 16785408 | tf_op jit(solution)/shard_map/gather | solution.py:259
  437.2 190.7 %all_to_all.32 = bf16[32,64,2048]{2,1,0:T(8,128)(2,1)S(1)} all-to-all(bf16[32,64,2048]{2,1,0:T(8,128)(2,1)} %bitcast.269), channel_id=1, replica_groups=mesh['sp'=32,'tp'=8] {'sp'}, dimensions={0} | all-to-all | bytes 16777216 | tf_op jit(solution)/shard_map/all_to_all | solution.py:260
  632.4 5.2 multiply_convert_fusion
  637.6 6.8 convolution_convert_fusion
  644.4 5.8 all-to-all-start.3
  650.7 30.7 %scatter_custom_fusion.1 = f32[2048]{0:T(1024)S(1)} fusion(s32[8192]{0:T(1024)S(1)} %bitcast.285, f32[8192]{0:T(1024)S(1)} %reshape.1357, f32[]{:T(128)} %constant.86.clone.1), kind=kCustom, calls=%fused_computation.412 | custom fusion | bytes 8196 | tf_op jit(solution)/shard_map/scatter | solution.py:256
  685.0 8.0 fusion.91
  693.0 137.3 %all-to-all-done.3 = bf16[32,64,2048]{2,1,0:T(8,128)(2,1)} async-done(((bf16[32,64,2048]{2,1,0:T(8,128)(2,1)}), bf16[32,64,2048]{2,1,0:T(8,128)(2,1)}, u32[]{:S(2)}, u32[]{:S(2)}) %all-to-all-start.3) | async-done | bytes 8388640 | tf_op jit(solution)/shard_map/all_to_all | solution.py:268
  830.3 34.7 %scatter_custom_fusion.2 = f32[1024,2048]{1,0:T(8,128)} fusion(f32[1024,2048]{1,0:T(8,128)} %fusion.91, s32[2048]{0:T(1024)S(1)} %get-tuple-element.132, bf16[2048,2048]{1,0:T(8,128)(2,1)} %bitcast.44, f32[2048]{0:T(1024)S(1)} %scatter_custom_fusion.1), kind=kCustom, calls=%fused_computation.5 | custom fusion | flops 12582912 | bytes 16785408 | tf_op jit(solution)/shard_map/scatter-add | solution.py:274
  865.0 6.0 convert_element_type.169
  871.1 45.4 %reduce-scatter.2.cloned.1.call-done = bf16[128,2048]{1,0:T(8,128)(2,1)} async-done(((bf16[1024,2048]{1,0:T(8,128)(2,1)}), bf16[128,2048]{1,0:T(8,128)(2,1)}) %reduce-scatter.2.cloned.1.call-update) | async-done | bytes 524304 | tf_op jit(solution)/shard_map/reduce_scatter | solution.py:283
  (552 shorter events, 221.9 us)
Async XLA Ops:
  6.5 631.0 %copy-start = (bf16[1,512,2048]{2,1,0:T(8,128)(2,1)S(1)}, bf16[1,512,2048]{2,1,0:T(8,128)(2,1)}, u32[]{:S(2)}) copy-start(bf16[1,512,2048]{2,1,0:T(8,128)(2,1)} %param.34) | copy-start | bytes 6291460
  86.2 9.6 %slice-start.8 = ((f32[64,16,8]{2,0,1:T(8,128)}), f32[64,10,8]{2,0,1:T(8,128)S(1)}, s32[]{:S(2)}) async-start(f32[64,16,8]{2,0,1:T(8,128)} %copy-done.4), calls=%async_computation.15 | async-start | bytes 655360 | tf_op jit(solution)/shard_map/slice | solution.py:84
  86.2 9.6 %slice-start.9 = ((f32[64,16,8]{2,0,1:T(8,128)}), f32[64,11,8]{2,0,1:T(8,128)S(1)}, s32[]{:S(2)}) async-start(f32[64,16,8]{2,0,1:T(8,128)} %copy-done.4), calls=%async_computation.16 | async-start | bytes 720896 | tf_op jit(solution)/shard_map/slice | solution.py:84
  86.2 9.6 %slice-start.10 = ((f32[64,16,8]{2,0,1:T(8,128)}), f32[64,12,8]{2,0,1:T(8,128)S(1)}, s32[]{:S(2)}) async-start(f32[64,16,8]{2,0,1:T(8,128)} %copy-done.4), calls=%async_computation.17 | async-start | bytes 786432 | tf_op jit(solution)/shard_map/slice | solution.py:84
  110.1 9.2 copy-start.23
  110.1 9.2 copy-start.24
  110.2 9.2 copy-start.25
  110.2 9.2 copy-start.26
  110.2 9.2 copy-start.27
  110.2 9.2 copy-start.28
  153.0 37.2 %copy-start.53 = (pred[64,16]{0,1:T(8,128)(4,1)S(1)}, pred[64,16]{0,1:T(8,128)(4,1)}, u32[]{:S(2)}) copy-start(pred[64,16]{0,1:T(8,128)(4,1)} %get-tuple-element.113) | copy-start | bytes 3076
  252.6 80.1 %copy-start.14 = (f32[16,8,64]{2,1,0:T(8,128)S(1)}, f32[16,8,64]{2,1,0:T(8,128)}, u32[]{:S(2)}) copy-start(f32[16,8,64]{2,1,0:T(8,128)} %copy-done.13) | copy-start | bytes 98308
  254.3 28.5 %all-to-all-start = ((f32[32,6,512]{2,1,0:T(8,128)}), f32[32,6,512]{2,1,0:T(8,128)}, u32[]{:S(2)}, u32[]{:S(2)}) async-start(f32[32,6,512]{2,1,0:T(8,128)} %broadcast_in_dim.456), calls=%async_computation | async-start | bytes 1048576 | tf_op jit(solution)/shard_map/all_to_all | solution.py:13
  265.9 147.3 %all-gather.2.cloned.1.call-start = ((), (), s32[]{:S(2)}) async-start(), calls=%async_computation.5 | async-start | bytes 4718592 | tf_op jit(solution)/shard_map/all_gather | solution.py:232
  343.2 14.4 %copy-start.10 = (bf16[1024,2048]{1,0:T(8,128)(2,1)S(1)}, bf16[1024,2048]{1,0:T(8,128)(2,1)}, u32[]{:S(2)}) copy-start(bf16[1024,2048]{1,0:T(8,128)(2,1)} %param.28) | copy-start | bytes 12582916
  343.2 14.4 %copy-start.15 = (bf16[128,2048]{1,0:T(8,128)(2,1)S(1)}, bf16[128,2048]{1,0:T(8,128)(2,1)}, u32[]{:S(2)}) copy-start(bf16[128,2048]{1,0:T(8,128)(2,1)} %param.19) | copy-start | bytes 1572868
  345.8 13.7 %copy-start.50 = (f32[2048]{0:T(1024)S(1)}, f32[2048]{0:T(1024)}, u32[]{:S(2)}) copy-start(f32[2048]{0:T(1024)} %param.29) | copy-start | bytes 24580
  437.2 190.7 %copy-start.57 = (bf16[1,2048,512]{2,1,0:T(8,128)(2,1)S(1)}, bf16[1,2048,512]{2,1,0:T(8,128)(2,1)}, u32[]{:S(2)}) copy-start(bf16[1,2048,512]{2,1,0:T(8,128)(2,1)} %param.32) | copy-start | bytes 6291460
  644.4 37.0 %copy-start.16 = (bf16[2048,64]{0,1:T(8,128)(2,1)S(1)}, bf16[2048,64]{0,1:T(8,128)(2,1)}, u32[]{:S(2)}) copy-start(bf16[2048,64]{0,1:T(8,128)(2,1)} %param.35) | copy-start | bytes 786436
  644.4 185.9 %all-to-all-start.3 = ((bf16[32,64,2048]{2,1,0:T(8,128)(2,1)}), bf16[32,64,2048]{2,1,0:T(8,128)(2,1)}, u32[]{:S(2)}, u32[]{:S(2)}) async-start(bf16[32,64,2048]{2,1,0:T(8,128)(2,1)} %bitcast.270), calls=%async_computation.3 | async-start | bytes 16777216 | tf_op jit(solution)/shard_map/all_to_all | solution.py:268
  650.1 34.8 %copy-start.17 = (bf16[64,2048]{1,0:T(8,128)(2,1)S(1)}, bf16[64,2048]{1,0:T(8,128)(2,1)}, u32[]{:S(2)}) copy-start(bf16[64,2048]{1,0:T(8,128)(2,1)} %param.37) | copy-start | bytes 786436
  650.1 34.8 %copy-start.18 = (bf16[2048,64]{0,1:T(8,128)(2,1)S(1)}, bf16[2048,64]{0,1:T(8,128)(2,1)}, u32[]{:S(2)}) copy-start(bf16[2048,64]{0,1:T(8,128)(2,1)} %param.36) | copy-start | bytes 786436
  650.1 266.3 %reduce-scatter.2.cloned.1.call-start = ((), (), s32[]{:S(2)}) async-start(), calls=%async_computation.6 | async-start | bytes 4718592 | tf_op jit(solution)/shard_map/reduce_scatter | solution.py:283
  871.1 45.4 %copy-start.8 = (f32[128,2048]{1,0:T(8,128)S(1)}, f32[128,2048]{1,0:T(8,128)}, u32[]{:S(2)}) copy-start(f32[128,2048]{1,0:T(8,128)} %copy-done.7) | copy-start | bytes 3145732
  (50 other events, 336.0 us)
Sparse Core Ops, SparseCore 0:
  360.5 29.4 all-gather.1
  871.2 45.1 reduce-scatter.1
where the time goes:
time: 940 us; the launch traced here: 926 us
  local copies, waits for them, and re-layouts  262 us (28%)
  blocking collectives  202 us (21%)
  waiting for transfers between devices  200 us (21%)
  other arithmetic  188 us (20%)
  matrix products  35.4 us (4%)
  between operations  21.2 us (2%)
  starting transfers between devices  17.5 us (2%)
    all_to_all x1, blocking collectives, body(): lax.all_to_all(outbound, 'sp', split_axis=0, concat_axis=0, tiled=True)  191 us
    all_to_all x1, waiting for transfers between devices, body(): lax.all_to_all(expert_rows.reshape(arrived.shape), 'sp', split_axis=0, co...  137 us
    slice x56, local copies, waits for them, and re-layouts, shift_down(): return jnp.pad(values[:, :values.shape[1] - lag], widths)  56.4 us
    reduce_scatter x1, waiting for transfers between devices, body(): lax.psum_scatter(partial_value.astype(jnp.bfloat16), 'tp', scatter_dimens...  45.4 us
    scatter-add x1, other arithmetic, body(): routed = jnp.zeros((token_count, model_width), jnp.float32).at[token_tabl...  34.7 us
    add x1, other arithmetic, blocked_states(): acc_im = acc_im + coef_re * src_im + coef_im * src_re  33.5 us
    sub x1, other arithmetic, blocked_states(): acc_re = acc_re + coef_re * src_re - coef_im * src_im  33.4 us
    scatter x1, local copies, waits for them, and re-layouts, body(): weight_table = jnp.zeros((sp_count * capacity,), jnp.float32).at[slot_ind...  30.7 us
  transfers between devices with their start and end apart: 4, of which 3 were waited for; matrix products, arithmetic and copies ran while one was open for 10% of the time, Pallas kernels for 0%

commit v1 on v0

v1 whole, which is shorter than its diff:
```python
import functools
import jax
import jax.numpy as jnp
from jax import lax
from jax.experimental import pallas as pl
from jax.experimental.pallas import tpu as pltpu
from jax.sharding import Mesh, PartitionSpec as P

norm_eps = 1e-06
highest = lax.Precision.HIGHEST
lanes_of_blocks = 8
reach = 4


def expand_gain(gain_ref, states):
    groups = gain_ref.shape[1]
    wide = groups * states
    lane_group = lax.broadcasted_iota(jnp.int32, (groups, wide), 1) // states
    row_group = lax.broadcasted_iota(jnp.int32, (groups, wide), 0)
    spread = jnp.where(lane_group == row_group, 1.0, 0.0).astype(jnp.float32)
    return jnp.dot(gain_ref[...], spread, precision=highest, preferred_element_type=jnp.float32)


def drive(input_ref, map_ref, scale_ref, gain_ref, driven, gain, states):
    rows = input_ref.shape[0]
    order_row = lax.broadcasted_iota(jnp.int32, (rows, rows), 0)
    order_col = lax.broadcasted_iota(jnp.int32, (rows, rows), 1)
    steps = rows // lanes_of_blocks
    source = (order_row % lanes_of_blocks) * steps + order_row // lanes_of_blocks
    pick = jnp.where(source == order_col, 1.0, 0.0).astype(jnp.bfloat16)
    stepped = jnp.dot(pick, input_ref[...], preferred_element_type=jnp.float32).astype(jnp.bfloat16)
    driven[...] = (
        jnp.dot(stepped, map_ref[...], preferred_element_type=jnp.float32) * scale_ref[...]
    )
    gain[...] = expand_gain(gain_ref, states)


def block_summary(states, input_ref, map_ref, scale_ref, gain_ref, turn_ref, out_ref, driven, gain):
    drive(input_ref, map_ref, scale_ref, gain_ref, driven, gain, states)
    wide = turn_ref.shape[1]
    steps = input_ref.shape[0] // lanes_of_blocks
    shape = (lanes_of_blocks, wide)
    turn_re = jnp.broadcast_to(turn_ref[0:1], shape)
    turn_im = jnp.broadcast_to(turn_ref[1:2], shape)

    def one(step, held):
        p_re, p_im, s_re, s_im = held
        rows = pl.ds(pl.multiple_of(step * lanes_of_blocks, lanes_of_blocks), lanes_of_blocks)
        g = gain[rows, :]
        a_re = g * turn_re
        a_im = g * turn_im
        return (
            a_re * p_re - a_im * p_im,
            a_re * p_im + a_im * p_re,
            a_re * s_re - a_im * s_im + driven[rows, :wide],
            a_re * s_im + a_im * s_re + driven[rows, wide:],
        )

    ones = jnp.ones(shape, jnp.float32)
    zero = jnp.zeros(shape, jnp.float32)
    last = lax.fori_loop(0, steps, one, (ones, zero, zero, zero), unroll=4)
    for k in range(4):
        out_ref[k] = last[k]


def read_out(
    states, input_ref, map_ref, scale_ref, gain_ref, turn_ref, enter_ref, readout_ref, skip_ref,
    out_ref, driven, gain,
):
    drive(input_ref, map_ref, scale_ref, gain_ref, driven, gain, states)
    wide = turn_ref.shape[1]
    rows_all = input_ref.shape[0]
    steps = rows_all // lanes_of_blocks
    shape = (lanes_of_blocks, wide)
    turn_re = jnp.broadcast_to(turn_ref[0:1], shape)
    turn_im = jnp.broadcast_to(turn_ref[1:2], shape)

    def one(step, held):
        s_re, s_im = held
        rows = pl.ds(pl.multiple_of(step * lanes_of_blocks, lanes_of_blocks), lanes_of_blocks)
        g = gain[rows, :]
        a_re = g * turn_re
        a_im = g * turn_im
        n_re = a_re * s_re - a_im * s_im + driven[rows, :wide]
        n_im = a_re * s_im + a_im * s_re + driven[rows, wide:]
        driven[rows, :wide] = n_re
        driven[rows, wide:] = n_im
        return n_re, n_im

    lax.fori_loop(0, steps, one, (enter_ref[0], enter_ref[1]), unroll=4)
    full = driven[...]
    high = full.astype(jnp.bfloat16)
    low = (full - high.astype(jnp.float32)).astype(jnp.bfloat16)
    stepped = jnp.dot(high, readout_ref[...], preferred_element_type=jnp.float32) + jnp.dot(
        low, readout_ref[...], preferred_element_type=jnp.float32
    )
    s_high = stepped.astype(jnp.bfloat16)
    s_low = (stepped - s_high.astype(jnp.float32)).astype(jnp.bfloat16)
    order_row = lax.broadcasted_iota(jnp.int32, (rows_all, rows_all), 0)
    order_col = lax.broadcasted_iota(jnp.int32, (rows_all, rows_all), 1)
    source = (order_row % steps) * lanes_of_blocks + order_row // steps
    pick = jnp.where(source == order_col, 1.0, 0.0).astype(jnp.bfloat16)
    natural = jnp.dot(pick, s_high, preferred_element_type=jnp.float32) + jnp.dot(
        pick, s_low, preferred_element_type=jnp.float32
    )
    natural = natural + skip_ref[...] * input_ref[...].astype(jnp.float32)
    out_ref[...] = jax.nn.gelu(natural).astype(jnp.bfloat16)


vmem = pl.BlockSpec(memory_space=pltpu.VMEM)


def mixer(mixer_input, document_ids, decay_rate, rotation, forget_log, input_map, readout_map, skip_gain):
    rows, channels = mixer_input.shape
    groups, states = decay_rate.shape
    size = channels // groups
    wide = groups * states
    steps = rows // lanes_of_blocks
    own = jnp.eye(groups, dtype=jnp.bfloat16)
    map_wide = jnp.einsum("cgph,gk->ghckp", input_map, own).reshape(channels, 2 * wide)
    readout_wide = jnp.einsum(
        "cghp,gk->cgpkh", readout_map * jnp.array([1, -1], jnp.bfloat16)[:, None, None, None], own
    ).reshape(2 * wide, channels)
    scale = jnp.sqrt(1.0 - jnp.exp(-2.0 * decay_rate)).reshape(1, wide)
    scale = jnp.concatenate([scale, scale], axis=1)
    magnitude = jnp.exp(-decay_rate)
    turn = jnp.stack(
        [(magnitude * jnp.cos(rotation)).reshape(-1), (magnitude * jnp.sin(rotation)).reshape(-1)]
    )
    starts = jnp.concatenate([jnp.zeros((1,), bool), document_ids[1:] != document_ids[:-1]])
    gain = jnp.where(starts[:, None], 0.0, jnp.exp(forget_log))
    gain = gain.reshape(lanes_of_blocks, steps, groups).transpose(1, 0, 2).reshape(rows, groups)
    skip = skip_gain.reshape(1, channels)
    scratch = [pltpu.VMEM((rows, 2 * wide), jnp.float32), pltpu.VMEM((rows, wide), jnp.float32)]
    params = pltpu.CompilerParams(vmem_limit_bytes=48 * 1024 * 1024)
    ends = pl.pallas_call(
        functools.partial(block_summary, states),
        out_shape=jax.ShapeDtypeStruct((4, lanes_of_blocks, wide), jnp.float32),
        in_specs=[vmem] * 5,
        out_specs=vmem,
        scratch_shapes=scratch,
        compiler_params=params,
        name="block_summary",
    )(mixer_input, map_wide, scale, gain, turn)

    p_re, p_im, s_re, s_im = ends
    a_re, a_im = jnp.ones((wide,), jnp.float32), jnp.zeros((wide,), jnp.float32)
    b_re, b_im = jnp.zeros((wide,), jnp.float32), jnp.zeros((wide,), jnp.float32)
    for k in range(lanes_of_blocks):
        a_re, a_im = p_re[k] * a_re - p_im[k] * a_im, p_re[k] * a_im + p_im[k] * a_re
        b_re, b_im = (
            p_re[k] * b_re - p_im[k] * b_im + s_re[k],
            p_re[k] * b_im + p_im[k] * b_re + s_im[k],
        )
    first_doc = document_ids[0].astype(jnp.float32)
    last_doc = document_ids[-1].astype(jnp.float32)
    first_row = jnp.full((wide,), 1.0, jnp.float32) * first_doc
    last_row = jnp.full((wide,), 1.0, jnp.float32) * last_doc
    summary = jnp.stack([a_re, a_im, b_re, b_im, first_row, last_row, first_row, last_row])
    shards = lax.axis_size("z") * lax.axis_size("x")
    me = lax.axis_index("z") * lax.axis_size("x") + lax.axis_index("x")
    earlier = [
        lax.ppermute(summary, ("z", "x"), [(i, (i + k) % shards) for i in range(shards)])
        for k in range(1, reach + 1)
    ]
    e_re, e_im = jnp.zeros((wide,), jnp.float32), jnp.zeros((wide,), jnp.float32)
    for k in range(reach, 0, -1):
        before = earlier[k - 1]
        t_re = before[0] * e_re - before[1] * e_im + before[2]
        t_im = before[0] * e_im + before[1] * e_re + before[3]
        after = earlier[k - 2][4] if k > 1 else first_row
        joined = (before[5] == after) & (me >= k)
        e_re = jnp.where(joined, t_re, 0.0)
        e_im = jnp.where(joined, t_im, 0.0)
    enter = []
    for k in range(lanes_of_blocks):
        enter.append((e_re, e_im))
        e_re, e_im = (
            p_re[k] * e_re - p_im[k] * e_im + s_re[k],
            p_re[k] * e_im + p_im[k] * e_re + s_im[k],
        )
    enter = jnp.stack([jnp.stack([e[0] for e in enter]), jnp.stack([e[1] for e in enter])])
    return pl.pallas_call(
        functools.partial(read_out, states),
        out_shape=jax.ShapeDtypeStruct((rows, channels), jnp.bfloat16),
        in_specs=[vmem] * 8,
        out_specs=vmem,
        scratch_shapes=scratch,
        compiler_params=params,
        name="read_out",
    )(mixer_input, map_wide, scale, gain, turn, enter, readout_wide, skip)


def body(
    stream,
    mixer_input,
    document_ids,
    decay_rate,
    rotation,
    forget_log,
    input_map,
    readout_map,
    skip_gain,
    out_projection,
    norm_gain,
    expert_ids,
    route_weight,
    expert_gate,
    expert_up,
    expert_down,
    shared_gate,
    shared_up,
    shared_down,
):
    column = lax.axis_index("tp")
    plane = lax.axis_index("z")
    peers = lax.axis_size("x") * lax.axis_size("tp")
    token_count, route_count = expert_ids.shape
    capacity = max(2, 2 * token_count * route_count // (lax.axis_size("z") * peers))

    gate_all = lax.all_gather(shared_gate, "tp", axis=1, tiled=True)
    up_all = lax.all_gather(shared_up, "tp", axis=1, tiled=True)
    down_all = lax.all_gather(shared_down, "tp", axis=0, tiled=True)
    ids_t = lax.all_gather(expert_ids.T, "z")
    weight_t = lax.all_gather(route_weight.T, "z")
    ids_t = lax.dynamic_index_in_dim(ids_t, column, 0, keepdims=False)
    weight_t = lax.dynamic_index_in_dim(weight_t, column, 0, keepdims=False)
    local = ids_t - plane * peers
    named = local[None] == jnp.arange(peers, dtype=jnp.int32)[:, None, None]
    member = jnp.any(named, axis=1)
    member_weight = jnp.sum(jnp.where(named, weight_t[None], 0.0), axis=1)
    spot = jnp.arange(token_count, dtype=jnp.int32)
    ahead = (spot[:, None] < spot[None, :]).astype(jnp.bfloat16)
    rank = jnp.dot(member.astype(jnp.bfloat16), ahead, preferred_element_type=jnp.float32)
    rank = jnp.where(member, rank.astype(jnp.int32), -1)
    slot = jnp.arange(capacity, dtype=jnp.int32)
    chosen = rank[:, None, :] == slot[None, :, None]
    pick = chosen.astype(jnp.bfloat16).reshape(peers * capacity, token_count)
    spread = (
        jnp.where(chosen, member_weight[:, None, :], 0.0)
        .astype(jnp.bfloat16)
        .reshape(peers * capacity, token_count)
    )

    mixer_out = mixer(
        mixer_input, document_ids, decay_rate, rotation, forget_log, input_map, readout_map, skip_gain
    )
    whole_rows = lax.all_to_all(mixer_out, "tp", split_axis=0, concat_axis=1, tiled=True)
    mixed = jnp.dot(whole_rows, out_projection, preferred_element_type=jnp.float32)
    residual = (stream.astype(jnp.float32) + mixed).astype(jnp.bfloat16)
    resid_f = residual.astype(jnp.float32)
    normed = (
        resid_f
        * lax.rsqrt(jnp.mean(resid_f * resid_f, axis=-1, keepdims=True) + norm_eps)
        * norm_gain[None, :]
    ).astype(jnp.bfloat16)
    model_width = normed.shape[1]

    gathered = lax.all_gather(normed, "z")
    tokens = lax.all_to_all(gathered, "tp", split_axis=0, concat_axis=0, tiled=True)
    tokens = tokens.reshape(token_count, model_width)
    rows = jnp.dot(pick, tokens, preferred_element_type=jnp.float32).astype(jnp.bfloat16)
    arrived = lax.all_to_all(
        rows.reshape(peers, capacity, model_width), ("x", "tp"), split_axis=0, concat_axis=0, tiled=True
    )
    row_block = arrived.reshape(-1, model_width)
    gate_value = jnp.dot(row_block, expert_gate[0], preferred_element_type=jnp.float32)
    up_value = jnp.dot(row_block, expert_up[0], preferred_element_type=jnp.float32)
    hidden = (jax.nn.silu(gate_value) * up_value).astype(jnp.bfloat16)
    expert_rows = jnp.dot(hidden, expert_down[0], preferred_element_type=jnp.float32).astype(
        jnp.bfloat16
    )
    returned = lax.all_to_all(
        expert_rows.reshape(arrived.shape), ("x", "tp"), split_axis=0, concat_axis=0, tiled=True
    )
    gate_block = jnp.dot(normed, gate_all, preferred_element_type=jnp.float32)
    up_block = jnp.dot(normed, up_all, preferred_element_type=jnp.float32)
    shared_hidden = (jax.nn.silu(gate_block) * up_block).astype(jnp.bfloat16)
    shared = jnp.dot(shared_hidden, down_all, preferred_element_type=jnp.float32)

    plane_sum = lax.dot_general(
        spread,
        returned.reshape(-1, model_width),
        (((0,), (0,)), ((), ())),
        preferred_element_type=jnp.float32,
    ).astype(jnp.bfloat16)
    back = lax.all_to_all(
        plane_sum.reshape(gathered.shape), "tp", split_axis=0, concat_axis=0, tiled=True
    )
    routed = lax.psum_scatter(back, "z", scatter_dimension=0, tiled=False)
    return (resid_f + shared + routed.astype(jnp.float32)).astype(jnp.bfloat16)


def solution(mesh):
    devices = mesh.devices
    planes = devices.shape[1]
    shape = (planes, devices.shape[0] // planes, devices.shape[1])
    split = Mesh(devices.reshape(shape), ("z", "x", "tp"))
    sp = ("z", "x")
    every = ("z", "x", "tp")
    placed = (
        P(every, None),
        P(sp, "tp"),
        P(sp),
        P("tp", None),
        P("tp", None),
        P(sp, "tp"),
        P(None, "tp", None, None),
        P(None, "tp", None, None),
        P("tp", None),
        P(),
        P(),
        P(sp, None),
        P(sp, None),
        P(every, None, None),
        P(every, None, None),
        P(every, None, None),
        P(None, "tp"),
        P(None, "tp"),
        P("tp", None),
    )
    return jax.shard_map(
        body, mesh=split, in_specs=placed, out_specs=P(every, None), check_vma=False
    )
```

time: 940 us -> 578 us (0.61)
  local copies, waits for them, and re-layouts: 262 us -> 10.1 us
  other arithmetic: 188 us -> 10.6 us
  waiting for transfers between devices: 200 us -> 273 us
  blocking collectives: 202 us -> 161 us
  starting transfers between devices: 17.5 us -> 33.8 us
  matrix products: 35.4 us -> 51.3 us
  Pallas kernels: 0 us -> 14.3 us
    slice x203 -> x1, local copies, waits for them, and re-layouts: 107 us -> 1.34 us  [mixer(): last_doc = document_ids[-1].astype(jnp.float32)]
    all_to_all x1, blocking collectives: 191 us -> 99.2 us  [body(): lax.all_to_all(rows.reshape(peers, capacity, model_width), ('x', 'tp'), s...]
    scatter x2 -> x0, local copies, waits for them, and re-layouts: 61.4 us -> none  [the longest x1 30.7 us: body(): weight_table = jnp.zeros((sp_count * capacity,), jnp.float32).at[slot_ind...]
    all_gather x1 -> x4, waiting for transfers between devices: 0.02 us -> 53.2 us  [the longest x1 53.1 us: body(): gathered = lax.all_gather(normed, 'z')]
    all_gather x0 -> x2, blocking collectives: none -> 50 us  [the longest x1 25 us: body(): weight_t = lax.all_gather(route_weight.T, 'z')]
    sub x6 -> x1, other arithmetic: 43.8 us -> 0.01 us  [mixer(): p_re[k] * a_re - p_im[k] * a_im]
    add x39 -> x8, other arithmetic: 42.8 us -> 0.85 us  [the longest x1 0.68 us: mixer(): p_re[k] * e_re - p_im[k] * e_im + s_re[k]]
    scatter-add x1 -> x0, other arithmetic: 34.7 us -> none  [body(): routed = jnp.zeros((token_count, model_width), jnp.float32).at[token_tabl...]
  transfers between devices with their start and end apart: 4 -> 12, of which waited for: 3 -> 5; matrix products, arithmetic and copies ran while one was open for 10% -> 4% of each run, Pallas kernels for 0% -> 0%
where the time goes in v1:
time: 578 us; the launch traced here: 571 us
  waiting for transfers between devices  273 us (47%)
  blocking collectives  161 us (28%)
  matrix products  51.3 us (9%)
  starting transfers between devices  33.8 us (6%)
  between operations  16.9 us (3%)
  Pallas kernels  14.3 us (2%)
  other arithmetic  10.6 us (2%)
  local copies, waits for them, and re-layouts  10.1 us (2%)
    all_to_all x1, blocking collectives, body(): lax.all_to_all(rows.reshape(peers, capacity, model_width), ('x', 'tp'), s...  99.2 us
    all_to_all x1, waiting for transfers between devices, body(): lax.all_to_all(expert_rows.reshape(arrived.shape), ('x', 'tp'), split_axi...  88.7 us
    all_to_all x1, waiting for transfers between devices, body(): lax.all_to_all(plane_sum.reshape(gathered.shape), 'tp', split_axis=0, con...  57.5 us
    all_gather x1, waiting for transfers between devices, body(): gathered = lax.all_gather(normed, 'z')  53.1 us
    reduce_scatter x1, waiting for transfers between devices, body(): routed = lax.psum_scatter(back, 'z', scatter_dimension=0, tiled=False)  50.2 us
    all_gather x1, blocking collectives, body(): weight_t = lax.all_gather(route_weight.T, 'z')  25 us
    all_gather x1, blocking collectives, body(): ids_t = lax.all_gather(expert_ids.T, 'z')  25 us
    all_to_all x1, waiting for transfers between devices, body(): lax.all_to_all(gathered, 'tp', split_axis=0, concat_axis=0, tiled=True)  21.3 us
  transfers between devices with their start and end apart: 12, of which 5 were waited for; matrix products, arithmetic and copies ran while one was open for 4% of the time, Pallas kernels for 0%

profile of v1, /device:TPU:4, one launch (start us, length us, event | category | flops | bytes accessed | tf_op | source)
XLA Modules:
  0.0 570.5 jit_solution(11308526121458078813)
XLA Ops:
  14.2 5.1 block_summary.1
  24.2 2.5 collective-permute-start.2
  36.8 9.2 %read_out.1 = bf16[1024,128]{1,0:T(8,128)(2,1)S(1)} custom-call(bf16[1024,128]{1,0:T(8,128)(2,1)S(1)} %copy-done.2, bf16[128,1024]{1,0:T(8,128)(2,1)S(1)} %reshape.1440.map_ref, f32[1,1024]{1,0:T(1,128)S(1)} %constant_dynamic-update-slice_fusion.scale_ref, f32[1024,8]{1,0:T(8,128)S(1)} %bitcast.468, f32[2,512]{1,0:T(2,128)S(1)} %pad_maximum_fusion.1.turn_ref, ...), custom_call_target="tpu_custom_call" | custom-call | tf_op jit(solution)/shard_map/read_out/pallas_call | solution.py:183
  47.8 11.8 %all_to_all.39 = bf16[8,128,128]{1,2,0:T(8,128)(2,1)S(1)} all-to-all(bf16[8,128,128]{1,2,0:T(8,128)(2,1)S(1)} %copy.35), channel_id=1, replica_groups=mesh['z'=8,'x'=4,'tp'=8] {'tp'}, dimensions={0} | all-to-all | bytes 524288 | tf_op jit(solution)/shard_map/all_to_all | solution.py:248
  59.6 3.1 multiply_reduce_fusion
  63.7 53.1 %all-gather.14.cloned.1.call-done = bf16[1024,2048]{1,0:T(8,128)(2,1)} async-done(((bf16[128,2048]{1,0:T(8,128)(2,1)}), bf16[1024,2048]{1,0:T(8,128)(2,1)}) %all-gather.14.cloned.1.call-update) | async-done | bytes 4194320 | tf_op jit(solution)/shard_map/all_gather | solution.py:259
  116.8 4.7 all-to-all-start.1
  121.5 25.0 %all-gather = s32[64,1024]{1,0:T(8,128)S(1)} all-gather(s32[8,1024]{1,0:T(8,128)S(1)} %bitcast.483), channel_id=2, replica_groups=mesh['z'=8,'x'=4,'tp'=8] {'z'}, dimensions={0}, use_global_device_ids=true | all-gather | bytes 294912 | tf_op jit(solution)/shard_map/all_gather | solution.py:224
  147.2 2.6 iota_compare_fusion
  149.8 21.3 %all-to-all-done.1 = bf16[8,128,2048]{2,1,0:T(8,128)(2,1)} async-done(((bf16[8,128,2048]{2,1,0:T(8,128)(2,1)}), bf16[8,128,2048]{2,1,0:T(8,128)(2,1)}, u32[]{:S(2)}, u32[]{:S(2)}) %all-to-all-start.1) | async-done | bytes 4194336 | tf_op jit(solution)/shard_map/all_to_all | solution.py:260
  171.1 11.5 %convolution_convert_fusion.1 = bf16[2048,2048]{1,0:T(8,128)(2,1)S(1)} fusion(pred[2048,1024]{1,0:T(32,128)(4,1)} %bitcast.476, bf16[1024,2048]{1,0:T(8,128)(2,1)} %bitcast.55), kind=kOutput, calls=%fused_computation.4 | convolution fusion | flops 8594128896 | bytes 14680064 | tf_op jit(solution)/shard_map/dot_general | solution.py:262
  182.7 99.2 %all_to_all.40 = bf16[32,64,2048]{2,1,0:T(8,128)(2,1)S(1)} all-to-all(bf16[32,64,2048]{2,1,0:T(8,128)(2,1)S(1)} %bitcast.471), channel_id=1, replica_groups=mesh['z'=8,'x'=4,'tp'=8] {'x','tp'}, dimensions={0} | all-to-all | bytes 16777216 | tf_op jit(solution)/shard_map/all_to_all | solution.py:263
  281.9 4.5 fusion.9
  286.4 5.2 multiply_convert_fusion
  291.6 6.7 %convolution_convert_fusion = bf16[2048,2048]{1,0:T(8,128)(2,1)} fusion(bf16[2048,512]{1,0:T(8,128)(2,1)S(1)} %multiply_convert_fusion, bf16[1,512,2048]{2,1,0:T(8,128)(2,1)S(1)} %copy-done), kind=kOutput, calls=%fused_computation.3 | convolution fusion | flops 4299161600 | bytes 12582912 | tf_op jit(solution)/shard_map/dot_general | solution.py:270
  298.4 7.0 %all-to-all-start.3 = ((bf16[32,64,2048]{2,1,0:T(8,128)(2,1)}), bf16[32,64,2048]{2,1,0:T(8,128)(2,1)}, u32[]{:S(2)}, u32[]{:S(2)}) async-start(bf16[32,64,2048]{2,1,0:T(8,128)(2,1)} %bitcast.470), calls=%async_computation.3 | async-start | bytes 16777216 | tf_op jit(solution)/shard_map/all_to_all | solution.py:273
  306.5 25.0 %all-gather.1 = f32[64,1024]{1,0:T(8,128)S(1)} all-gather(f32[8,1024]{1,0:T(8,128)S(1)} %bitcast.484), channel_id=3, replica_groups=mesh['z'=8,'x'=4,'tp'=8] {'z'}, dimensions={0}, use_global_device_ids=true | all-gather | bytes 294912 | tf_op jit(solution)/shard_map/all_gather | solution.py:225
  331.9 88.7 %all-to-all-done.3 = bf16[32,64,2048]{2,1,0:T(8,128)(2,1)} async-done(((bf16[32,64,2048]{2,1,0:T(8,128)(2,1)}), bf16[32,64,2048]{2,1,0:T(8,128)(2,1)}, u32[]{:S(2)}, u32[]{:S(2)}) %all-to-all-start.3) | async-done | bytes 8388640 | tf_op jit(solution)/shard_map/all_to_all | solution.py:273
  420.7 12.8 %bitcast_convert_fusion = bf16[1024,2048]{1,0:T(8,128)(2,1)} fusion(bf16[32,64,2048]{2,1,0:T(8,128)(2,1)} %all-to-all-done.3, bf16[32,1024]{1,0:T(8,128)(2,1)S(1)} %select_reduce_fusion, s32[32,1024]{1,0:T(8,128)} %copy-done.4), kind=kOutput, calls=%fused_computation | convolution fusion | flops 8596226048 | bytes 12779520 | tf_op jit(solution)/shard_map/dot_general | solution.py:281
  433.4 13.6 %all-to-all-start.4 = ((bf16[8,128,2048]{2,1,0:T(8,128)(2,1)}), bf16[8,128,2048]{2,1,0:T(8,128)(2,1)}, u32[]{:S(2)}, u32[]{:S(2)}) async-start(bf16[8,128,2048]{2,1,0:T(8,128)(2,1)} %bitcast.475), calls=%async_computation.4 | async-start | bytes 8388608 | tf_op jit(solution)/shard_map/all_to_all | solution.py:287
  447.7 57.5 %all-to-all-done.4 = bf16[8,128,2048]{2,1,0:T(8,128)(2,1)} async-done(((bf16[8,128,2048]{2,1,0:T(8,128)(2,1)}), bf16[8,128,2048]{2,1,0:T(8,128)(2,1)}, u32[]{:S(2)}, u32[]{:S(2)}) %all-to-all-start.4) | async-done | bytes 4194336 | tf_op jit(solution)/shard_map/all_to_all | solution.py:287
  505.3 2.6 fusion.41
  508.0 50.2 %reduce-scatter.2.cloned.1.call-done = bf16[1,128,2048]{2,1,0:T(8,128)(2,1)} async-done(((bf16[8,128,2048]{2,1,0:T(8,128)(2,1)}), bf16[1,128,2048]{2,1,0:T(8,128)(2,1)}) %reduce-scatter.2.cloned.1.call-update) | async-done | bytes 524304 | tf_op jit(solution)/shard_map/reduce_scatter | solution.py:290
  558.1 4.5 fusion.6
  (89 shorter events, 26.1 us)
Async XLA Ops:
  7.4 284.3 %copy-start = (bf16[1,512,2048]{2,1,0:T(8,128)(2,1)S(1)}, bf16[1,512,2048]{2,1,0:T(8,128)(2,1)}, u32[]{:S(2)}) copy-start(bf16[1,512,2048]{2,1,0:T(8,128)(2,1)} %param.35) | copy-start | bytes 6291460
  7.4 29.4 %copy-start.2 = (bf16[1024,128]{1,0:T(8,128)(2,1)S(1)}, bf16[1024,128]{1,0:T(8,128)(2,1)}, u32[]{:S(2)}) copy-start(bf16[1024,128]{1,0:T(8,128)(2,1)} %input_ref.3) | copy-start | bytes 786436
  7.4 26.8 %copy-start.8 = (f32[8,16]{1,0:T(8,128)S(1)}, f32[8,16]{1,0:T(8,128)}, u32[]{:S(2)}) copy-start(f32[8,16]{1,0:T(8,128)} %param.28) | copy-start | bytes 1540
  7.4 109.4 %all-gather.14.cloned.1.call-start = ((), (), s32[]{:S(2)}) async-start(), calls=%async_computation.10 | async-start | bytes 4718592 | tf_op jit(solution)/shard_map/all_gather | solution.py:259
  13.2 1.0 copy-start.1
  20.8 13.5 %collective-permute-start = (f32[8,512]{1,0:T(8,128)S(1)}, f32[8,512]{1,0:T(8,128)S(1)}, u32[]{:S(2)}, u32[]{:S(2)}) collective-permute-start(f32[8,512]{1,0:T(8,128)S(1)} %stack.21), channel_id=1, source_target_pairs={{0,8},{8,16},{16,24},{24,32},{32,40},{40,48},{48,56},{56,64},{64,7... | collective-permute-start | bytes 49160 | tf_op jit(solution)/shard_map/ppermute | solution.py:163
  22.0 12.3 %collective-permute-start.1 = (f32[8,512]{1,0:T(8,128)S(1)}, f32[8,512]{1,0:T(8,128)S(1)}, u32[]{:S(2)}, u32[]{:S(2)}) collective-permute-start(f32[8,512]{1,0:T(8,128)S(1)} %stack.21), channel_id=1, source_target_pairs={{0,16},{8,24},{16,32},{24,40},{32,48},{40,56},{48,64},{56,72},{64,... | collective-permute-start | bytes 49160 | tf_op jit(solution)/shard_map/ppermute | solution.py:163
  24.2 10.1 %collective-permute-start.2 = (f32[8,512]{1,0:T(8,128)S(1)}, f32[8,512]{1,0:T(8,128)S(1)}, u32[]{:S(2)}, u32[]{:S(2)}) collective-permute-start(f32[8,512]{1,0:T(8,128)S(1)} %stack.21), channel_id=1, source_target_pairs={{0,24},{8,32},{16,40},{24,48},{32,56},{40,64},{48,72},{56,80},{64,... | collective-permute-start | bytes 49160 | tf_op jit(solution)/shard_map/ppermute | solution.py:163
  26.7 7.6 %collective-permute-start.3 = (f32[8,512]{1,0:T(8,128)S(1)}, f32[8,512]{1,0:T(8,128)}, u32[]{:S(2)}, u32[]{:S(2)}) collective-permute-start(f32[8,512]{1,0:T(8,128)S(1)} %stack.21), channel_id=1, source_target_pairs={{0,32},{8,40},{16,48},{24,56},{32,64},{40,72},{48,80},{56,88},{64,... | collective-permute-start | bytes 49160 | tf_op jit(solution)/shard_map/ppermute | solution.py:163
  36.8 25.9 %copy-start.7 = (f32[2048]{0:T(1024)S(1)}, f32[2048]{0:T(1024)}, u32[]{:S(2)}) copy-start(f32[2048]{0:T(1024)} %param.30) | copy-start | bytes 24580
  46.0 0.7 copy-start.3
  116.8 4.7 copy-start.5
  116.8 54.3 %all-to-all-start.1 = ((bf16[8,128,2048]{2,1,0:T(8,128)(2,1)}), bf16[8,128,2048]{2,1,0:T(8,128)(2,1)}, u32[]{:S(2)}, u32[]{:S(2)}) async-start(bf16[8,128,2048]{2,1,0:T(8,128)(2,1)} %bitcast.474), calls=%async_computation.1 | async-start | bytes 8388608 | tf_op jit(solution)/shard_map/all_to_all | solution.py:260
  147.2 35.5 %copy-start.4 = (s32[32,1024]{1,0:T(8,128)}, s32[32,1024]{1,0:T(8,128)S(1)}, u32[]{:S(2)}) copy-start(s32[32,1024]{1,0:T(8,128)S(1)} %fusion.13) | copy-start | bytes 393220
  182.7 99.2 %copy-start.9 = (bf16[1,2048,512]{2,1,0:T(8,128)(2,1)S(1)}, bf16[1,2048,512]{2,1,0:T(8,128)(2,1)}, u32[]{:S(2)}) copy-start(bf16[1,2048,512]{2,1,0:T(8,128)(2,1)} %param.33) | copy-start | bytes 6291460
  281.9 4.5 copy-start.10
  298.4 8.2 %copy-start.6 = (f32[1024,8]{0,1:T(8,128)S(1)}, f32[1024,8]{0,1:T(8,128)}, u32[]{:S(2)}) copy-start(f32[1024,8]{0,1:T(8,128)} %param.32) | copy-start | bytes 98308
  298.4 122.3 %all-to-all-start.3 = ((bf16[32,64,2048]{2,1,0:T(8,128)(2,1)}), bf16[32,64,2048]{2,1,0:T(8,128)(2,1)}, u32[]{:S(2)}, u32[]{:S(2)}) async-start(bf16[32,64,2048]{2,1,0:T(8,128)(2,1)} %bitcast.470), calls=%async_computation.3 | async-start | bytes 16777216 | tf_op jit(solution)/shard_map/all_to_all | solution.py:273
  305.3 199.9 %all-gather.8.cloned.1.call-start = ((), (), s32[]{:S(2)}) async-start(), calls=%async_computation.6 | async-start | bytes 2359296 | tf_op jit(solution)/shard_map/all_gather | solution.py:221
  305.9 202.0 %all-gather.10.cloned.1.call-start = ((), (), s32[]{:S(2)}) async-start(), calls=%async_computation.7 | async-start | bytes 2359296 | tf_op jit(solution)/shard_map/all_gather | solution.py:222
  433.4 71.8 %all-to-all-start.4 = ((bf16[8,128,2048]{2,1,0:T(8,128)(2,1)}), bf16[8,128,2048]{2,1,0:T(8,128)(2,1)}, u32[]{:S(2)}, u32[]{:S(2)}) async-start(bf16[8,128,2048]{2,1,0:T(8,128)(2,1)} %bitcast.475), calls=%async_computation.4 | async-start | bytes 8388608 | tf_op jit(solution)/shard_map/all_to_all | solution.py:287
  447.1 60.9 %all-gather.12.cloned.1.call-start = ((), (), s32[]{:S(2)}) async-start(), calls=%async_computation.8 | async-start | bytes 2359296 | tf_op jit(solution)/shard_map/all_gather | solution.py:223
  447.6 110.5 %reduce-scatter.2.cloned.1.call-start = ((), (), s32[]{:S(2)}) async-start(), calls=%async_computation.9 | async-start | bytes 4718592 | tf_op jit(solution)/shard_map/reduce_scatter | solution.py:290
Sparse Core Ops, SparseCore 0:
  63.8 52.9 all-gather.13
  505.4 52.7 reduce-scatter.1
Sparse Core Ops, SparseCore 1:
  307.7 99.3 all-gather.7
  408.8 25.4 all-gather.9
  449.4 33.5 all-gather.11
